TPU v7x, 32 devices: a whole 2x2x4 slice. The times are simulated.
32 devices in a mesh: sp: 8 (over z, y), tp: 4 (over x, core).
Axes of the slice: x: 2, y: 2, z: 4, core: 2. Of those that a mesh axis runs over, the one named last changes fastest.
Arguments:
- hidden_states: bfloat16 [4096, 4096], P('sp', 'tp'), may hold values from -6 to 6
- pre_gain: float32 [2, 4096], replicated, may hold values from 0.1 to 1.9
- post_gain: float32 [2, 4096], P(None, 'tp'), may hold values from 0.1 to 1.9
- w_value: bfloat16 [2, 4096, 2048], P(None, 'sp', 'tp'), may hold values from -0.09375 to 0.09375
- w_outer: bfloat16 [2, 4096, 2048], P(None, 'sp', 'tp'), may hold values from -0.09375 to 0.09375
- w_inner: bfloat16 [2, 4096, 2048], P(None, 'sp', 'tp'), may hold values from -0.09375 to 0.09375
- taps: float32 [2, 3, 2048], P(None, None, 'tp'), may hold values from -3 to 3
- w_out: bfloat16 [2, 2048, 4096], P(None, 'tp', 'sp'), as said below
Outputs:
- final_states: bfloat16 [4096, 4096], P('sp', 'tp')
Inputs may be any that keep to these rules, and one draw needn't show every extreme that they name: `w_out`: independent entries; the columns fall into 8 groups of 512 consecutive columns, each group with its own scale.
All inputs are finite; a program needn't handle non-finite values.
Results may differ from a plain program's by a relative error of at most 0.024.
Values may be sent and summed in bfloat16 or wider, within the bound.
A program may use at most 128 MiB of HBM per device.

v0:
```python
import jax
import jax.numpy as jnp
from jax import lax
from jax.sharding import PartitionSpec as P

D = 4096
eps = 1e-06


def passed_along(value, axis, by):
    size = lax.axis_size(axis)
    pairs = [(i, i + by) for i in range(size) if 0 <= i + by < size]
    return lax.ppermute(value, axis, pairs)


def local(hidden_states, pre_gain, post_gain, w_value, w_outer, w_inner, taps, w_out):
    current = hidden_states
    layers = w_value.shape[0]
    whole_value, whole_outer, whole_inner, whole_out = (
        lax.all_gather(w_value, "sp", axis=1, tiled=True),
        lax.all_gather(w_outer, "sp", axis=1, tiled=True),
        lax.all_gather(w_inner, "sp", axis=1, tiled=True),
        lax.all_gather(w_out, "sp", axis=2, tiled=True),
    )
    for layer_index in range(layers):
        gathered = lax.all_gather(current, "tp", axis=1, tiled=True)
        widened = gathered.astype(jnp.float32)
        normed = (
            widened
            * lax.rsqrt(jnp.mean(widened * widened, axis=1, keepdims=True) + eps)
            * pre_gain[layer_index]
        ).astype(jnp.bfloat16)
        value_proj = jnp.dot(normed, whole_value[layer_index], preferred_element_type=jnp.float32)
        outer_proj = jnp.dot(normed, whole_outer[layer_index], preferred_element_type=jnp.float32)
        inner_proj = jnp.dot(normed, whole_inner[layer_index], preferred_element_type=jnp.float32)
        gated_input = (inner_proj * value_proj).astype(jnp.bfloat16)
        before = passed_along(gated_input[-2:], "sp", 1)
        extended = jnp.concatenate([before, gated_input], axis=0).astype(jnp.float32)
        length = gated_input.shape[0]
        kernel = taps[layer_index]
        convolved = (
            extended[0:length] * kernel[0]
            + extended[1 : length + 1] * kernel[1]
            + extended[2 : length + 2] * kernel[2]
        )
        conv_out = (outer_proj * convolved).astype(jnp.bfloat16)
        partial_terms = jnp.dot(
            conv_out, whole_out[layer_index], preferred_element_type=jnp.float32
        )
        mixed = lax.psum_scatter(
            partial_terms.astype(jnp.bfloat16), "tp", scatter_dimension=1, tiled=True
        ).astype(jnp.float32)
        power = lax.psum(jnp.sum(mixed * mixed, axis=1), "tp")
        rescale = lax.rsqrt(power / D + eps)
        current = (
            current.astype(jnp.float32) + mixed * rescale[:, None] * post_gain[layer_index]
        ).astype(jnp.bfloat16)
    return current


def solution(mesh):
    placed = (
        P("sp", "tp"),
        P(),
        P(None, "tp"),
        P(None, "sp", "tp"),
        P(None, "sp", "tp"),
        P(None, "sp", "tp"),
        P(None, None, "tp"),
        P(None, "tp", "sp"),
    )
    return jax.shard_map(
        local, mesh=mesh, in_specs=placed, out_specs=P("sp", "tp"), check_vma=False
    )
```

profile of v0, /device:TPU:0, one launch (start us, length us, event | category | flops | bytes accessed | tf_op | source)
XLA Modules:
  0.0 729.6 jit_solution(7224380522898905791)
XLA Ops:
  6.5 0.0 copy-start.3
  6.5 0.0 all-gather.7.cloned.1.call-start
  6.5 0.7 all-gather.7.cloned.1.call-update
  7.3 0.0 all-gather.13.cloned.1.call-start
  7.3 0.7 all-gather.13.cloned.1.call-update
  8.0 0.0 all-gather.11.cloned.1.call-start
  8.1 0.7 all-gather.11.cloned.1.call-update
  8.7 0.0 all-gather.9.cloned.1.call-start
  8.8 0.5 all-gather.9.cloned.1.call-update
  9.3 0.0 all-gather.15.cloned.1.call-start
  9.4 0.5 all-gather.15.cloned.1.call-update
  9.9 0.0 reduce-scatter.3.cloned.1.call-start
  10.0 0.0 copy-done.3
  10.0 36.1 %all-gather.7.cloned.1.call-done = bf16[512,4096]{1,0:T(8,128)(2,1)} async-done(((bf16[512,1024]{1,0:T(8,128)(2,1)}), bf16[512,4096]{1,0:T(8,128)(2,1)}) %all-gather.7.cloned.1.call-update) | async-done | bytes 4194320 | tf_op jit(solution)/shard_map/all_gather | solution.py:26
  46.1 3.1 fusion
  49.2 123.6 %all-gather.13.cloned.1.call-done = bf16[2,4096,512]{2,1,0:T(8,128)(2,1)} async-done(((bf16[2,512,512]{2,1,0:T(8,128)(2,1)}), bf16[2,4096,512]{2,1,0:T(8,128)(2,1)}) %all-gather.13.cloned.1.call-update) | async-done | bytes 8388624 | tf_op jit(solution)/shard_map/all_gather | solution.py:20
  172.8 5.8 fusion.9
  178.6 0.0 copy-start.4
  178.6 119.0 %all-gather.11.cloned.1.call-done = bf16[2,4096,512]{2,1,0:T(8,128)(2,1)} async-done(((bf16[2,512,512]{2,1,0:T(8,128)(2,1)}), bf16[2,4096,512]{2,1,0:T(8,128)(2,1)}) %all-gather.11.cloned.1.call-update) | async-done | bytes 8388624 | tf_op jit(solution)/shard_map/all_gather | solution.py:22
  297.6 5.8 fusion.26
  303.5 2.5 collective-permute-start
  306.0 0.0 copy-done.4
  306.0 1.3 collective-permute-done
  307.3 0.2 maximum_convert_fusion
  307.4 114.9 %all-gather.9.cloned.1.call-done = bf16[2,4096,512]{2,1,0:T(8,128)(2,1)} async-done(((bf16[2,512,512]{2,1,0:T(8,128)(2,1)}), bf16[2,4096,512]{2,1,0:T(8,128)(2,1)}) %all-gather.9.cloned.1.call-update) | async-done | bytes 8388624 | tf_op jit(solution)/shard_map/all_gather | solution.py:21
  422.4 6.0 fusion.27
  428.4 119.0 %all-gather.15.cloned.1.call-done = bf16[2,512,4096]{2,1,0:T(8,128)(2,1)} async-done(((bf16[2,512,512]{2,1,0:T(8,128)(2,1)}), bf16[2,512,4096]{2,1,0:T(8,128)(2,1)}) %all-gather.15.cloned.1.call-update) | async-done | bytes 8388624 | tf_op jit(solution)/shard_map/all_gather | solution.py:23
  547.4 6.7 convolution_convert_fusion.1
  554.1 0.0 copy-start.5
  554.1 0.0 copy-start.2
  554.1 0.0 reduce-scatter.3.cloned.1.call-update
  554.1 0.0 all-gather.17.cloned.1.call-start
  554.1 0.6 copy-done.5
  554.8 42.1 %reduce-scatter.3.cloned.1.call-done = bf16[512,1024]{1,0:T(8,128)(2,1)} async-done(((bf16[512,4096]{1,0:T(8,128)(2,1)}), bf16[512,1024]{1,0:T(8,128)(2,1)}) %reduce-scatter.3.cloned.1.call-update) | async-done | bytes 1048592 | tf_op jit(solution)/shard_map/reduce_scatter | solution.py:50
  596.8 1.5 fusion.12
  598.3 5.8 psum.14
  604.1 0.0 copy-done.2
  604.1 2.6 fusion.15
  606.7 0.0 all-gather.17.cloned.1.call-update
  606.8 0.2 reduce-scatter.5.cloned.1.call-start
  607.0 35.0 %all-gather.17.cloned.1.call-done = bf16[512,4096]{1,0:T(8,128)(2,1)} async-done(((bf16[512,1024]{1,0:T(8,128)(2,1)}), bf16[512,4096]{1,0:T(8,128)(2,1)}) %all-gather.17.cloned.1.call-update) | async-done | bytes 4194320 | tf_op jit(solution)/shard_map/all_gather | solution.py:26
  642.0 0.0 copy-start.1
  642.0 3.2 fusion.3
  645.2 0.2 copy-done.1
  645.4 0.0 slice-start.2
  645.4 4.7 fusion.6
  650.2 0.0 slice-start.3
  650.2 4.7 fusion.24
  655.0 3.4 collective-permute-start.1
  658.3 1.3 collective-permute-done.1
  659.6 0.2 maximum_convert_fusion.1
  659.8 0.0 slice-done.2
  659.8 0.0 slice-done.3
  659.8 0.0 slice-start.1
  659.8 2.6 fusion.25
  662.4 0.0 slice-done
  662.4 0.7 slice-done.1
  663.2 4.3 convolution_convert_fusion
  667.5 0.0 reduce-scatter.5.cloned.1.call-update
  667.5 45.4 %reduce-scatter.5.cloned.1.call-done = bf16[512,1024]{1,0:T(8,128)(2,1)} async-done(((bf16[512,4096]{1,0:T(8,128)(2,1)}), bf16[512,1024]{1,0:T(8,128)(2,1)}) %reduce-scatter.5.cloned.1.call-update) | async-done | bytes 1048592 | tf_op jit(solution)/shard_map/reduce_scatter | solution.py:50
  712.9 1.5 fusion.16
  714.4 5.8 psum.15
  720.1 0.0 copy-done
  720.1 2.6 fusion.19
  (13 shorter events, 0.1 us)
Async XLA Ops:
  6.5 3.4 copy-start.3
  6.5 39.6 %all-gather.7.cloned.1.call-start = ((), (), s32[]{:S(2)}) async-start(), calls=%async_computation.2 | async-start | bytes 5242880 | tf_op jit(solution)/shard_map/all_gather | solution.py:26
  7.3 165.5 %all-gather.13.cloned.1.call-start = ((), (), s32[]{:S(2)}) async-start(), calls=%async_computation.5 | async-start | bytes 9437184 | tf_op jit(solution)/shard_map/all_gather | solution.py:20
  8.0 289.6 %all-gather.11.cloned.1.call-start = ((), (), s32[]{:S(2)}) async-start(), calls=%async_computation.4 | async-start | bytes 9437184 | tf_op jit(solution)/shard_map/all_gather | solution.py:22
  8.7 413.6 %all-gather.9.cloned.1.call-start = ((), (), s32[]{:S(2)}) async-start(), calls=%async_computation.3 | async-start | bytes 9437184 | tf_op jit(solution)/shard_map/all_gather | solution.py:21
  9.3 538.1 %all-gather.15.cloned.1.call-start = ((), (), s32[]{:S(2)}) async-start(), calls=%async_computation.6 | async-start | bytes 9437184 | tf_op jit(solution)/shard_map/all_gather | solution.py:23
  9.9 586.9 %reduce-scatter.3.cloned.1.call-start = ((), (), s32[]{:S(2)}) async-start(), calls=%async_computation.7 | async-start | bytes 5242880 | tf_op jit(solution)/shard_map/reduce_scatter | solution.py:50
  178.6 127.4 %copy-start.4 = (f32[2,3,512]{2,0,1:T(2,128)S(1)}, f32[2,3,512]{2,0,1:T(2,128)}, u32[]{:S(2)}) copy-start(f32[2,3,512]{2,0,1:T(2,128)} %param.14) | copy-start | bytes 36868
  303.5 3.8 collective-permute-start
  554.1 0.7 copy-start.5
  554.1 50.0 %copy-start.2 = (bf16[512,1024]{1,0:T(8,128)(2,1)S(1)}, bf16[512,1024]{1,0:T(8,128)(2,1)}, u32[]{:S(2)}) copy-start(bf16[512,1024]{1,0:T(8,128)(2,1)} %param.8) | copy-start | bytes 3145732
  554.1 87.9 %all-gather.17.cloned.1.call-start = ((), (), s32[]{:S(2)}) async-start(), calls=%async_computation.8 | async-start | bytes 5242880 | tf_op jit(solution)/shard_map/all_gather | solution.py:26
  606.8 106.1 %reduce-scatter.5.cloned.1.call-start = ((), (), s32[]{:S(2)}) async-start(), calls=%async_computation.9 | async-start | bytes 5242880 | tf_op jit(solution)/shard_map/reduce_scatter | solution.py:50
  642.0 3.4 copy-start.1
  645.4 14.4 %slice-start.2 = ((s8[8388608]{0:T(1024)(128)(4,1)}), s8[4194304]{0:T(1024)(128)(4,1)S(1)}, s32[]{:S(2)}) async-start(s8[8388608]{0:T(1024)(128)(4,1)} %bitcast.68), calls=%async_computation.12 | async-start | bytes 8388608
  650.2 9.6 %slice-start.3 = ((s8[8388608]{0:T(1024)(128)(4,1)}), s8[4194304]{0:T(1024)(128)(4,1)S(1)}, s32[]{:S(2)}) async-start(s8[8388608]{0:T(1024)(128)(4,1)} %bitcast.68), calls=%async_computation.13 | async-start | bytes 8388608
  655.0 4.7 collective-permute-start.1
  659.6 2.8 slice-start
  659.8 3.3 slice-start.1
  667.5 52.7 %copy-start = (bf16[512,1024]{1,0:T(8,128)(2,1)S(1)}, bf16[512,1024]{1,0:T(8,128)(2,1)}, u32[]{:S(2)}) copy-start(bf16[512,1024]{1,0:T(8,128)(2,1)} %fusion.15) | copy-start | bytes 3145732
Sparse Core Ops, SparseCore 0:
  8.9 37.1 all-gather.6
  48.3 124.4 all-gather.12
  175.0 122.6 all-gather.10
  299.7 122.6 all-gather.8
  424.2 123.1 all-gather.14
  554.2 42.5 reduce-scatter.2
  606.9 35.0 all-gather.16
  667.6 45.2 reduce-scatter.4
where the time goes:
time: 730 us
  waiting for transfers between devices  641 us (88%)
  matrix products  40.7 us (6%)
  other arithmetic  14.9 us (2%)
  between operations  13.7 us (2%)
  blocking collectives  11.5 us (2%)
    all_gather x1, waiting for transfers between devices, local(): lax.all_gather(w_value, 'sp', axis=1, tiled=True)  124 us
    all_gather x1, waiting for transfers between devices, local(): lax.all_gather(w_out, 'sp', axis=2, tiled=True)  119 us
    all_gather x1, waiting for transfers between devices, local(): lax.all_gather(w_inner, 'sp', axis=1, tiled=True)  119 us
    all_gather x1, waiting for transfers between devices, local(): lax.all_gather(w_outer, 'sp', axis=1, tiled=True)  115 us
    reduce_scatter x2, waiting for transfers between devices, local(): lax.psum_scatter(partial_terms.astype(jnp.bfloat16), 'tp', scatter_dimens...  87.4 us
    all_gather x2, waiting for transfers between devices, local(): gathered = lax.all_gather(current, 'tp', axis=1, tiled=True)  71.1 us
  transfers between devices with their start and end apart: 10, of which 10 were waited for; matrix products, arithmetic and copies ran while one was open for 3% of the time, Pallas kernels for 0%

commit v1 on v0

--- a/solution.py
+++ b/solution.py
@@ -23,7 +23,14 @@
         lax.all_gather(w_out, "sp", axis=2, tiled=True),
     )
     for layer_index in range(layers):
-        gathered = lax.all_gather(current, "tp", axis=1, tiled=True)
+        ring = [current]
+        for hop in range(3):
+            ring.append(lax.ppermute(ring[-1], "tp", [(dev, (dev + 1) % 4) for dev in range(4)]))
+        gathered = jnp.roll(
+            jnp.concatenate(ring[::-1], axis=1),
+            (lax.axis_index("tp") + 1) * ring[0].shape[1],
+            axis=1,
+        )
         widened = gathered.astype(jnp.float32)
         normed = (
             widened

time: 730 us -> 703 us (0.963)
  waiting for transfers between devices: 641 us -> 607 us
  other arithmetic: 14.9 us -> 23.3 us
    ppermute x0 -> x6, waiting for transfers between devices: none -> 84.8 us  [local(): lax.ppermute(ring[-1], 'tp', [(dev, (dev + 1) % 4) for dev in range(4)])]
    all_gather x2 -> x0, waiting for transfers between devices: 71.1 us -> none  [local(): gathered = lax.all_gather(current, 'tp', axis=1, tiled=True)]
    all_gather x1, waiting for transfers between devices: 124 us -> 75.5 us  [local(): lax.all_gather(w_value, 'sp', axis=1, tiled=True)]
    reduce_sum x2, other arithmetic: 6.31 us -> 15.7 us  [local(): jnp.mean(widened * widened, axis=1, keepdims=True) + eps]
  transfers between devices with their start and end apart: 10 -> 14, of which waited for: 10 -> 14; matrix products, arithmetic and copies ran while one was open for 3% -> 4% of each run, Pallas kernels for 0% -> 0%
where the time goes in v1:
time: 703 us; the launch traced here: 702 us
  waiting for transfers between devices  607 us (86%)
  matrix products  38.2 us (5%)
  other arithmetic  23.3 us (3%)
  between operations  13.7 us (2%)
  blocking collectives  11.5 us (2%)
    all_gather x1, waiting for transfers between devices, local(): lax.all_gather(w_out, 'sp', axis=2, tiled=True)  119 us
    all_gather x1, waiting for transfers between devices, local(): lax.all_gather(w_inner, 'sp', axis=1, tiled=True)  119 us
    all_gather x1, waiting for transfers between devices, local(): lax.all_gather(w_outer, 'sp', axis=1, tiled=True)  115 us
    reduce_scatter x2, waiting for transfers between devices, local(): lax.psum_scatter(partial_terms.astype(jnp.bfloat16), 'tp', scatter_dimens...  88.5 us
    ppermute x6, waiting for transfers between devices, local(): lax.ppermute(ring[-1], 'tp', [(dev, (dev + 1) % 4) for dev in range(4)])  84.8 us
    all_gather x1, waiting for transfers between devices, local(): lax.all_gather(w_value, 'sp', axis=1, tiled=True)  75.5 us
    reduce_sum x2, other arithmetic, local(): jnp.mean(widened * widened, axis=1, keepdims=True) + eps  15.7 us
  transfers between devices with their start and end apart: 14, of which 14 were waited for; matrix products, arithmetic and copies ran while one was open for 4% of the time, Pallas kernels for 0%

profile of v1, /device:TPU:0, one launch (start us, length us, event | category | flops | bytes accessed | tf_op | source)
XLA Modules:
  0.0 702.4 jit_solution(18023685906502437581)
XLA Ops:
  6.5 0.0 all-gather.9.cloned.1.call-start
  6.5 0.7 all-gather.9.cloned.1.call-update
  7.3 0.0 all-gather.7.cloned.1.call-start
  7.3 0.7 all-gather.7.cloned.1.call-update
  8.0 0.0 all-gather.5.cloned.1.call-start
  8.1 0.7 all-gather.5.cloned.1.call-update
  8.7 0.0 all-gather.11.cloned.1.call-start
  8.8 0.5 all-gather.11.cloned.1.call-update
  9.3 0.0 reduce-scatter.3.cloned.1.call-start
  9.4 0.5 collective-permute-start
  9.9 14.6 %collective-permute-done = bf16[512,1024]{1,0:T(8,128)(2,1)S(1)} collective-permute-done((bf16[512,1024]{1,0:T(8,128)(2,1)}, bf16[512,1024]{1,0:T(8,128)(2,1)S(1)}, u32[]{:S(2)}, u32[]{:S(2)}) %collective-permute-start) | collective-permute-done | bytes 1048608 | tf_op jit(solution)/shard_map/ppermute | solution.py:28
  24.5 0.0 collective-permute-start.1
  24.6 14.2 %collective-permute-done.1 = bf16[512,1024]{1,0:T(8,128)(2,1)S(1)} collective-permute-done((bf16[512,1024]{1,0:T(8,128)(2,1)S(1)}, bf16[512,1024]{1,0:T(8,128)(2,1)S(1)}, u32[]{:S(2)}, u32[]{:S(2)}) %collective-permute-start.1) | collective-permute-done | bytes 1048608 | tf_op jit(solution)/shard_map/ppermute | solution.py:28
  38.7 0.0 collective-permute-start.2
  38.7 0.9 fusion.54
  39.6 13.4 %collective-permute-done.2 = bf16[512,1024]{1,0:T(8,128)(2,1)S(1)} collective-permute-done((bf16[512,1024]{1,0:T(8,128)(2,1)S(1)}, bf16[512,1024]{1,0:T(8,128)(2,1)S(1)}, u32[]{:S(2)}, u32[]{:S(2)}) %collective-permute-start.2) | collective-permute-done | bytes 1048608 | tf_op jit(solution)/shard_map/ppermute | solution.py:28
  53.0 8.2 %fusion = (f32[512]{0:T(512)S(1)}, bf16[512,4096]{1,0:T(8,128)(2,1)}) fusion(s32[]{:T(128)S(6)} %select_n.13, bf16[512,1024]{1,0:T(8,128)(2,1)} %param.10, bf16[512,1024]{1,0:T(8,128)(2,1)S(1)} %collective-permute-done, bf16[512,1024]{1,0:T(8,128)(2,1)S(1)} %collective-permute-done.1, bf16[512,1024]{1,0:T(8,128)(2,1)S(1)} %collective-permute-done.2), kind=kLoop, calls=%fused_computation.4 | loop fusion | flops 39845376 | bytes 8390660 | tf_op jit(solution)/shard_map/reduce_sum | solution.py:37
  61.2 75.5 %all-gather.9.cloned.1.call-done = bf16[2,4096,512]{2,1,0:T(8,128)(2,1)} async-done(((bf16[2,512,512]{2,1,0:T(8,128)(2,1)}), bf16[2,4096,512]{2,1,0:T(8,128)(2,1)}) %all-gather.9.cloned.1.call-update) | async-done | bytes 8388624 | tf_op jit(solution)/shard_map/all_gather | solution.py:20
  136.7 5.8 fusion.23
  142.6 0.0 copy-start.1
  142.6 119.0 %all-gather.7.cloned.1.call-done = bf16[2,4096,512]{2,1,0:T(8,128)(2,1)} async-done(((bf16[2,512,512]{2,1,0:T(8,128)(2,1)}), bf16[2,4096,512]{2,1,0:T(8,128)(2,1)}) %all-gather.7.cloned.1.call-update) | async-done | bytes 8388624 | tf_op jit(solution)/shard_map/all_gather | solution.py:22
  261.6 5.8 fusion.40
  267.4 2.5 collective-permute-start.3
  269.9 0.0 copy-done.1
  269.9 1.3 collective-permute-done.3
  271.2 0.2 maximum_convert_fusion
  271.4 115.1 %all-gather.5.cloned.1.call-done = bf16[2,4096,512]{2,1,0:T(8,128)(2,1)} async-done(((bf16[2,512,512]{2,1,0:T(8,128)(2,1)}), bf16[2,4096,512]{2,1,0:T(8,128)(2,1)}) %all-gather.5.cloned.1.call-update) | async-done | bytes 8388624 | tf_op jit(solution)/shard_map/all_gather | solution.py:21
  386.4 6.0 fusion.41
  392.5 0.0 copy-start.2
  392.5 0.0 copy-start
  392.5 119.0 %all-gather.11.cloned.1.call-done = bf16[2,512,4096]{2,1,0:T(8,128)(2,1)} async-done(((bf16[2,512,512]{2,1,0:T(8,128)(2,1)}), bf16[2,512,4096]{2,1,0:T(8,128)(2,1)}) %all-gather.11.cloned.1.call-update) | async-done | bytes 8388624 | tf_op jit(solution)/shard_map/all_gather | solution.py:23
  511.5 6.6 convolution_convert_fusion.1
  518.1 0.0 reduce-scatter.3.cloned.1.call-update
  518.1 0.0 reduce-scatter.5.cloned.1.call-start
  518.2 0.0 copy-done.2
  518.2 42.7 %reduce-scatter.3.cloned.1.call-done = bf16[512,1024]{1,0:T(8,128)(2,1)} async-done(((bf16[512,4096]{1,0:T(8,128)(2,1)}), bf16[512,1024]{1,0:T(8,128)(2,1)}) %reduce-scatter.3.cloned.1.call-update) | async-done | bytes 1048592 | tf_op jit(solution)/shard_map/reduce_scatter | solution.py:57
  560.9 1.5 fusion.26
  562.4 5.8 psum.14
  568.1 0.0 copy-done
  568.1 1.7 fusion.29
  569.8 0.1 collective-permute-start.4
  569.9 14.2 %collective-permute-done.4 = bf16[512,1024]{1,0:T(8,128)(2,1)S(1)} collective-permute-done((bf16[512,1024]{1,0:T(8,128)(2,1)S(1)}, bf16[512,1024]{1,0:T(8,128)(2,1)S(1)}, u32[]{:S(2)}, u32[]{:S(2)}) %collective-permute-start.4) | collective-permute-done | bytes 1048608 | tf_op jit(solution)/shard_map/ppermute | solution.py:28
  584.1 0.0 collective-permute-start.5
  584.1 14.2 %collective-permute-done.5 = bf16[512,1024]{1,0:T(8,128)(2,1)S(1)} collective-permute-done((bf16[512,1024]{1,0:T(8,128)(2,1)S(1)}, bf16[512,1024]{1,0:T(8,128)(2,1)S(1)}, u32[]{:S(2)}, u32[]{:S(2)}) %collective-permute-start.5) | collective-permute-done | bytes 1048608 | tf_op jit(solution)/shard_map/ppermute | solution.py:28
  598.3 0.0 collective-permute-start.6
  598.3 14.2 %collective-permute-done.6 = bf16[512,1024]{1,0:T(8,128)(2,1)S(1)} collective-permute-done((bf16[512,1024]{1,0:T(8,128)(2,1)S(1)}, bf16[512,1024]{1,0:T(8,128)(2,1)S(1)}, u32[]{:S(2)}, u32[]{:S(2)}) %collective-permute-start.6) | collective-permute-done | bytes 1048608 | tf_op jit(solution)/shard_map/ppermute | solution.py:28
  612.5 7.4 %fusion.3 = (f32[512]{0:T(512)S(1)}, bf16[512,4096]{1,0:T(8,128)(2,1)S(1)}) fusion(s32[]{:T(128)S(6)} %select_n.13, bf16[512,1024]{1,0:T(8,128)(2,1)S(1)} %fusion.29, bf16[512,1024]{1,0:T(8,128)(2,1)S(1)} %collective-permute-done.4, bf16[512,1024]{1,0:T(8,128)(2,1)S(1)} %collective-permute-done.5, bf16[512,1024]{1,0:T(8,128)(2,1)S(1)} %collective-permute-done.6), kind=kLoop, calls=%fused_computation.7 | loop fusion | flops 39845376 | bytes 8390660 | tf_op jit(solution)/shard_map/reduce_sum | solution.py:37
  620.0 0.0 slice-start.5
  620.0 0.0 slice-start.2
  620.0 4.7 fusion.20
  624.7 0.0 slice-start.3
  624.8 2.4 fusion.38
  627.1 3.6 collective-permute-start.7
  630.7 1.3 collective-permute-done.7
  632.0 0.2 maximum_convert_fusion.1
  632.2 0.0 slice-start.1
  632.2 2.5 fusion.39
  634.8 0.8 slice-done.1
  635.5 4.3 convolution_convert_fusion
  639.8 0.0 reduce-scatter.5.cloned.1.call-update
  639.9 45.8 %reduce-scatter.5.cloned.1.call-done = bf16[512,1024]{1,0:T(8,128)(2,1)} async-done(((bf16[512,4096]{1,0:T(8,128)(2,1)}), bf16[512,1024]{1,0:T(8,128)(2,1)}) %reduce-scatter.5.cloned.1.call-update) | async-done | bytes 1048592 | tf_op jit(solution)/shard_map/reduce_scatter | solution.py:57
  685.7 1.5 fusion.30
  687.2 5.8 psum.15
  692.9 2.6 fusion.33
  (18 shorter events, 0.1 us)
Async XLA Ops:
  6.5 130.2 %all-gather.9.cloned.1.call-start = ((), (), s32[]{:S(2)}) async-start(), calls=%async_computation.4 | async-start | bytes 9437184 | tf_op jit(solution)/shard_map/all_gather | solution.py:20
  7.3 254.3 %all-gather.7.cloned.1.call-start = ((), (), s32[]{:S(2)}) async-start(), calls=%async_computation.3 | async-start | bytes 9437184 | tf_op jit(solution)/shard_map/all_gather | solution.py:22
  8.0 378.4 %all-gather.5.cloned.1.call-start = ((), (), s32[]{:S(2)}) async-start(), calls=%async_computation.2 | async-start | bytes 9437184 | tf_op jit(solution)/shard_map/all_gather | solution.py:21
  8.7 502.8 %all-gather.11.cloned.1.call-start = ((), (), s32[]{:S(2)}) async-start(), calls=%async_computation.5 | async-start | bytes 9437184 | tf_op jit(solution)/shard_map/all_gather | solution.py:23
  9.3 551.6 %reduce-scatter.3.cloned.1.call-start = ((), (), s32[]{:S(2)}) async-start(), calls=%async_computation.6 | async-start | bytes 5242880 | tf_op jit(solution)/shard_map/reduce_scatter | solution.py:57
  9.4 15.2 %collective-permute-start = (bf16[512,1024]{1,0:T(8,128)(2,1)}, bf16[512,1024]{1,0:T(8,128)(2,1)S(1)}, u32[]{:S(2)}, u32[]{:S(2)}) collective-permute-start(bf16[512,1024]{1,0:T(8,128)(2,1)} %param.10), channel_id=1, source_target_pairs={{0,1},{1,2},{2,3},{3,0},{4,5},{5,6},{6,7},{7,4},{8,9},{9,10},{10,1... | collective-permute-start | bytes 3145736 | tf_op jit(solution)/shard_map/ppermute | solution.py:28
  24.5 14.2 %collective-permute-start.1 = (bf16[512,1024]{1,0:T(8,128)(2,1)S(1)}, bf16[512,1024]{1,0:T(8,128)(2,1)S(1)}, u32[]{:S(2)}, u32[]{:S(2)}) collective-permute-start(bf16[512,1024]{1,0:T(8,128)(2,1)S(1)} %collective-permute-done), channel_id=1, source_target_pairs={{0,1},{1,2},{2,3},{3,0},{4,5},{5,6},{6,7},{7,4},{8,9},{9,10},{10,1... | collective-permute-start | bytes 3145736 | tf_op jit(solution)/shard_map/ppermute | solution.py:28
  38.7 14.2 %collective-permute-start.2 = (bf16[512,1024]{1,0:T(8,128)(2,1)S(1)}, bf16[512,1024]{1,0:T(8,128)(2,1)S(1)}, u32[]{:S(2)}, u32[]{:S(2)}) collective-permute-start(bf16[512,1024]{1,0:T(8,128)(2,1)S(1)} %collective-permute-done.1), channel_id=1, source_target_pairs={{0,1},{1,2},{2,3},{3,0},{4,5},{5,6},{6,7},{7,4},{8,9},{9,10},{10,1... | collective-permute-start | bytes 3145736 | tf_op jit(solution)/shard_map/ppermute | solution.py:28
  142.6 127.3 %copy-start.1 = (f32[2,3,512]{2,0,1:T(2,128)S(1)}, f32[2,3,512]{2,0,1:T(2,128)}, u32[]{:S(2)}) copy-start(f32[2,3,512]{2,0,1:T(2,128)} %param.16) | copy-start | bytes 36868
  267.4 3.8 collective-permute-start.3
  392.5 125.7 %copy-start.2 = (f32[2,1024]{1,0:T(2,128)S(1)}, f32[2,1024]{1,0:T(2,128)}, u32[]{:S(2)}) copy-start(f32[2,1024]{1,0:T(2,128)} %param.12) | copy-start | bytes 24580
  392.5 175.7 %copy-start = (bf16[512,1024]{1,0:T(8,128)(2,1)S(1)}, bf16[512,1024]{1,0:T(8,128)(2,1)}, u32[]{:S(2)}) copy-start(bf16[512,1024]{1,0:T(8,128)(2,1)} %param.10) | copy-start | bytes 3145732
  518.1 167.5 %reduce-scatter.5.cloned.1.call-start = ((), (), s32[]{:S(2)}) async-start(), calls=%async_computation.7 | async-start | bytes 5242880 | tf_op jit(solution)/shard_map/reduce_scatter | solution.py:57
  569.8 14.3 %collective-permute-start.4 = (bf16[512,1024]{1,0:T(8,128)(2,1)S(1)}, bf16[512,1024]{1,0:T(8,128)(2,1)S(1)}, u32[]{:S(2)}, u32[]{:S(2)}) collective-permute-start(bf16[512,1024]{1,0:T(8,128)(2,1)S(1)} %fusion.29), channel_id=1, source_target_pairs={{0,1},{1,2},{2,3},{3,0},{4,5},{5,6},{6,7},{7,4},{8,9},{9,10},{10,1... | collective-permute-start | bytes 3145736 | tf_op jit(solution)/shard_map/ppermute | solution.py:28
  584.1 14.2 %collective-permute-start.5 = (bf16[512,1024]{1,0:T(8,128)(2,1)S(1)}, bf16[512,1024]{1,0:T(8,128)(2,1)S(1)}, u32[]{:S(2)}, u32[]{:S(2)}) collective-permute-start(bf16[512,1024]{1,0:T(8,128)(2,1)S(1)} %collective-permute-done.4), channel_id=1, source_target_pairs={{0,1},{1,2},{2,3},{3,0},{4,5},{5,6},{6,7},{7,4},{8,9},{9,10},{10,1... | collective-permute-start | bytes 3145736 | tf_op jit(solution)/shard_map/ppermute | solution.py:28
  598.3 14.2 %collective-permute-start.6 = (bf16[512,1024]{1,0:T(8,128)(2,1)S(1)}, bf16[512,1024]{1,0:T(8,128)(2,1)S(1)}, u32[]{:S(2)}, u32[]{:S(2)}) collective-permute-start(bf16[512,1024]{1,0:T(8,128)(2,1)S(1)} %collective-permute-done.5), channel_id=1, source_target_pairs={{0,1},{1,2},{2,3},{3,0},{4,5},{5,6},{6,7},{7,4},{8,9},{9,10},{10,1... | collective-permute-start | bytes 3145736 | tf_op jit(solution)/shard_map/ppermute | solution.py:28
  612.5 12.2 %slice-start.4 = ((s8[8388608]{0:T(1024)(128)(4,1)}), s8[4194304]{0:T(1024)(128)(4,1)S(1)}, s32[]{:S(2)}) async-start(s8[8388608]{0:T(1024)(128)(4,1)} %bitcast.70), calls=%async_computation.12 | async-start | bytes 8388608
  620.0 4.7 slice-start.5
  620.0 12.2 %slice-start.2 = ((s8[8388608]{0:T(1024)(128)(4,1)}), s8[4194304]{0:T(1024)(128)(4,1)S(1)}, s32[]{:S(2)}) async-start(s8[8388608]{0:T(1024)(128)(4,1)} %bitcast.68), calls=%async_computation.10 | async-start | bytes 8388608
  624.7 7.5 %slice-start.3 = ((s8[8388608]{0:T(1024)(128)(4,1)}), s8[4194304]{0:T(1024)(128)(4,1)S(1)}, s32[]{:S(2)}) async-start(s8[8388608]{0:T(1024)(128)(4,1)} %bitcast.68), calls=%async_computation.11 | async-start | bytes 8388608
  627.1 4.9 collective-permute-start.7
  632.0 2.7 slice-start
  632.2 3.3 slice-start.1
Sparse Core Ops, SparseCore 0:
  9.5 127.1 all-gather.8
  138.9 122.6 all-gather.6
  263.8 122.6 all-gather.4
  388.3 123.1 all-gather.10
  518.3 42.5 reduce-scatter.2
  640.0 45.6 reduce-scatter.4
